TPU v7x, 256 devices: a whole 4x4x8 slice. The times are simulated.
256 devices in a mesh: ep: 16 (over y, x), tp: 16 (over z, core).
Axes of the slice: x: 4, y: 4, z: 8, core: 2. Of those that a mesh axis runs over, the one named last changes fastest.
Arguments:
- query_latent: bfloat16 [8192, 1024], P('ep'), may hold values from -6 to 6
- joint_latent: bfloat16 [8192, 512], P('ep'), may hold values from -6 to 6
- rotary_key: bfloat16 [8192, 32], P('ep'), may hold values from -60 to 60
- query_gain: float32 [1024], replicated, may hold values from 0.1 to 1.9
- joint_gain: float32 [512], replicated, may hold values from 0.1 to 1.9
- query_weight: bfloat16 [1024, 2048], P(None, 'tp'), may hold values from -0.1875 to 0.1875
- query_rotary: bfloat16 [1024, 1024], P(None, 'tp'), may hold values from -0.1875 to 0.1875
- key_weight: bfloat16 [512, 2048], P(None, 'tp'), may hold values from -0.25 to 0.25
- value_weight: bfloat16 [512, 2048], P(None, 'tp'), may hold values from -0.25 to 0.25
- output_weight: bfloat16 [2048, 2048], P('tp'), may hold values from -6 to 6
- expert_input: bfloat16 [8192, 2048], P('ep'), may hold values from -6 to 6
- expert_gain: float32 [2048], replicated, may hold values from 0.1 to 1.9
- routes: int32 [8192, 2], P('ep'), may hold values from 0 to 31, all different within a row; in each aligned block of 512 rows (0 to 511, 512 to 1023, ...) at most 48 rows name the same one
- route_weight: float32 [8192, 2], P('ep'), may hold values from 0.2 to 1
- gate_weight: bfloat16 [32, 2048, 4096], P('ep', None, 'tp'), may hold values from -0.125 to 0.125
- up_weight: bfloat16 [32, 2048, 4096], P('ep', None, 'tp'), may hold values from -0.125 to 0.125
- down_weight: bfloat16 [32, 4096, 2048], P('ep', 'tp'), may hold values from -0.09375 to 0.09375
Outputs:
- mixer_out: bfloat16 [8192, 2048], P(('ep', 'tp'))
- expert_out: bfloat16 [8192, 2048], P('ep', 'tp')
Inputs may be any that keep to these rules, and one draw needn't show every extreme that they name: `routes`: A row names 2 different experts. Among the rows of one device (aligned blocks of 512 rows) no expert is named by more than 48 rows, a bound that some block reaches.
All inputs are finite; a program needn't handle non-finite values.
Results may differ from a plain program's by a relative error of at most 0.019.
The roundings to bfloat16 on the way count: a program that leaves them out, or rounds other values in their place, can miss the bound.
Values may be sent and summed in bfloat16 or wider, within the bound.
A program may use at most 128 MiB of HBM per device.

v0:
```python
import jax
import jax.numpy as jnp
from jax import lax
from jax.sharding import PartitionSpec as P

NOPE = 64
VDIM = 64
NORM_EPSILON = 1e-06
ROTARY_BASE = 10000.0


def sent_together(arrays, axis, dim, along):
    both = jnp.concatenate(arrays, axis=along)
    out, at, outs = (lax.all_gather(both, axis, axis=dim, tiled=True), 0, [])
    for a in arrays:
        outs.append(lax.slice_in_dim(out, at, at + a.shape[along], axis=along))
        at += a.shape[along]
    return tuple(outs)


def norm_rows(source, gain_vector):
    as_float = source.astype(jnp.float32)
    factor = lax.rsqrt(jnp.mean(as_float * as_float, axis=-1, keepdims=True) + NORM_EPSILON)
    return (as_float * factor * gain_vector).astype(jnp.bfloat16)


def rotate(source, positions):
    half_width = source.shape[-1] // 2
    frequencies = ROTARY_BASE ** (-jnp.arange(half_width, dtype=jnp.float32) / half_width)
    angles = positions[:, None] * frequencies[None, :]
    view_shape = (source.shape[0],) + (1,) * (source.ndim - 2) + (half_width,)
    cosine_table = jnp.cos(angles).reshape(view_shape)
    sine_table = jnp.sin(angles).reshape(view_shape)
    first_half = source[..., :half_width]
    second = source[..., half_width:]
    return jnp.concatenate(
        [
            first_half * cosine_table - second * sine_table,
            second * cosine_table + first_half * sine_table,
        ],
        axis=-1,
    )


def attend_block(
    carried, query_plain, query_turned, key_block, value_block, turned_block, score_scale
):
    row_top, row_total, mixed_values = carried
    scores = jnp.einsum("qhd,khd->qhk", query_plain, key_block, preferred_element_type=jnp.float32)
    scores = scores + jnp.einsum(
        "qhd,kd->qhk", query_turned, turned_block, preferred_element_type=jnp.float32
    )
    scores = scores * score_scale
    new_top = jnp.maximum(row_top, jnp.max(scores, axis=-1))
    factor = jnp.exp(row_top - new_top)
    expo = jnp.exp(scores - new_top[..., None])
    row_total = row_total * factor + jnp.sum(expo, axis=-1)
    mixed_values = mixed_values * factor[..., None] + jnp.einsum(
        "qhk,khd->qhd", expo.astype(jnp.bfloat16), value_block, preferred_element_type=jnp.float32
    )
    return (new_top, row_total, mixed_values)


def token_mixer(
    query_latent,
    joint_latent,
    rotary_key,
    query_gain,
    joint_gain,
    query_weight,
    query_rotary,
    key_weight,
    value_weight,
    output_weight,
):
    row_count = query_latent.shape[0]
    head_count = key_weight.shape[1] // NOPE
    turn_width = rotary_key.shape[1]
    offset = lax.axis_index("ep") * row_count
    positions = (offset + jnp.arange(row_count, dtype=jnp.int32)).astype(jnp.float32)
    query_normed = norm_rows(query_latent, query_gain)
    joint_normed = norm_rows(joint_latent, joint_gain)
    turned_key = rotate(rotary_key.astype(jnp.float32), positions).astype(jnp.bfloat16)
    query_plain = jnp.dot(query_normed, query_weight, preferred_element_type=jnp.float32).astype(
        jnp.bfloat16
    )
    query_plain = query_plain.reshape(row_count, head_count, NOPE)
    query_turned = jnp.dot(query_normed, query_rotary, preferred_element_type=jnp.float32)
    query_turned = rotate(
        query_turned.reshape(row_count, head_count, turn_width), positions
    ).astype(jnp.bfloat16)
    score_scale = (NOPE + turn_width) ** (-0.5)
    start_carry = (
        jnp.full((row_count, head_count), -jnp.inf, jnp.float32),
        jnp.zeros((row_count, head_count), jnp.float32),
        jnp.zeros((row_count, head_count, VDIM), jnp.float32),
    )
    carried = start_carry
    latent_piece, turned_piece = sent_together((joint_normed, turned_key), "ep", 0, 1)
    block_rows = min(row_count, latent_piece.shape[0])
    block_total = latent_piece.shape[0] // block_rows

    def scan_step(inner_carry, key_items):
        latent_block, turned_block = key_items
        key_block = jnp.dot(latent_block, key_weight, preferred_element_type=jnp.float32)
        key_block = key_block.astype(jnp.bfloat16).reshape(block_rows, head_count, NOPE)
        value_block = jnp.dot(latent_block, value_weight, preferred_element_type=jnp.float32)
        value_block = value_block.astype(jnp.bfloat16).reshape(block_rows, head_count, VDIM)
        return (
            attend_block(
                inner_carry,
                query_plain,
                query_turned,
                key_block,
                value_block,
                turned_block,
                score_scale,
            ),
            None,
        )

    carried, _ = lax.scan(
        scan_step,
        carried,
        (
            latent_piece.reshape(block_total, block_rows, latent_piece.shape[1]),
            turned_piece.reshape(block_total, block_rows, turn_width),
        ),
    )
    row_top, row_total, mixed_values = carried
    attended = (
        (mixed_values / row_total[..., None])
        .astype(jnp.bfloat16)
        .reshape(row_count, head_count * VDIM)
    )
    return lax.psum_scatter(
        jnp.dot(attended, output_weight, preferred_element_type=jnp.float32).astype(jnp.bfloat16),
        "tp",
        scatter_dimension=0,
        tiled=True,
    )


def experts(expert_input, expert_gain, routes, route_weight, gate_weight, up_weight, down_weight):
    row_count = expert_input.shape[0]
    feature_width = expert_input.shape[1]
    top_count = routes.shape[1]
    group_count = lax.axis_size("ep")
    local_count = gate_weight.shape[0]
    expert_count = local_count * group_count
    capacity = 3 * row_count // (2 * group_count)
    part_width = feature_width // lax.axis_size("tp")
    flat_routes = routes.reshape(-1)
    onehot = (flat_routes[:, None] == jnp.arange(expert_count, dtype=jnp.int32)[None, :]).astype(
        jnp.int32
    )
    rank_within = jnp.sum((jnp.cumsum(onehot, axis=0) - onehot) * onehot, axis=1)
    slot_index = flat_routes * capacity + rank_within
    owner_token = jnp.arange(row_count * top_count, dtype=jnp.int32) // top_count
    slot_token = jnp.zeros((expert_count * capacity,), jnp.int32).at[slot_index].set(owner_token)
    filled = jnp.zeros((expert_count * capacity,), jnp.bfloat16).at[slot_index].set(1.0)
    normed = norm_rows(expert_input, expert_gain)
    columns = lax.dynamic_slice_in_dim(normed, lax.axis_index("tp") * part_width, part_width, 1)
    outgoing = (columns[slot_token] * filled[:, None]).reshape(
        group_count, local_count, capacity, part_width
    )
    arrived = lax.all_to_all(outgoing, "ep", split_axis=0, concat_axis=0, tiled=True)
    piece = lax.all_gather(arrived, "tp", axis=3, tiled=True)
    gate_running = jnp.einsum(
        "secd,edf->secf", piece, gate_weight, preferred_element_type=jnp.float32
    )
    up_running = jnp.einsum("secd,edf->secf", piece, up_weight, preferred_element_type=jnp.float32)
    hidden = (jax.nn.silu(gate_running) * up_running).astype(jnp.bfloat16)
    partial_value = jnp.einsum(
        "secf,efd->secd", hidden, down_weight, preferred_element_type=jnp.float32
    )
    summed = lax.psum_scatter(
        partial_value.astype(jnp.bfloat16), "tp", scatter_dimension=3, tiled=True
    )
    returned = lax.all_to_all(summed, "ep", split_axis=0, concat_axis=0, tiled=True)
    picked = returned.reshape(expert_count * capacity, part_width)[slot_index]
    picked = picked.astype(jnp.float32).reshape(row_count, top_count, part_width)
    return jnp.sum(picked * route_weight[:, :, None], axis=1).astype(jnp.bfloat16)


def local(
    query_latent,
    joint_latent,
    rotary_key,
    query_gain,
    joint_gain,
    query_weight,
    query_rotary,
    key_weight,
    value_weight,
    output_weight,
    expert_input,
    expert_gain,
    routes,
    route_weight,
    gate_weight,
    up_weight,
    down_weight,
):
    mixer_out = token_mixer(
        query_latent,
        joint_latent,
        rotary_key,
        query_gain,
        joint_gain,
        query_weight,
        query_rotary,
        key_weight,
        value_weight,
        output_weight,
    )
    expert_out = experts(
        expert_input, expert_gain, routes, route_weight, gate_weight, up_weight, down_weight
    )
    return (mixer_out, expert_out)


def solution(mesh):
    return jax.shard_map(
        local,
        mesh=mesh,
        in_specs=(
            P("ep", None),
            P("ep", None),
            P("ep", None),
            P(),
            P(),
            P(None, "tp"),
            P(None, "tp"),
            P(None, "tp"),
            P(None, "tp"),
            P("tp", None),
            P("ep", None),
            P(),
            P("ep", None),
            P("ep", None),
            P("ep", None, "tp"),
            P("ep", None, "tp"),
            P("ep", "tp", None),
        ),
        out_specs=(P(("ep", "tp"), None), P("ep", "tp")),
        check_vma=False,
    )
```

profile of v0, /device:TPU:6, one launch (start us, length us, event | category | flops | bytes accessed | tf_op | source)
XLA Modules:
  0.0 353.4 jit_solution(10818710300028206992)
XLA Ops:
  7.2 4.2 %convert_element_type.83 = f32[512,2048]{1,0:T(8,128)} convert(bf16[512,2048]{1,0:T(8,128)(2,1)} %param.29) | non-fusion elementwise | flops 1048576 | bytes 6291456 | tf_op jit(solution)/shard_map/convert_element_type | solution.py:22
  12.7 9.0 %reduce-window.6 = s32[32,8,128]{2,1,0:T(8,128)S(1)} reduce-window(s32[32,8,128]{2,1,0:T(8,128)S(1)} %fusion.46, s32[]{:T(128)} %constant.30.clone.1), window={size=1x1x128 pad=0_0x0_0x127_0}, to_apply=%region_8.9 | reduce-window | flops 4161536 | bytes 262148 | tf_op jit(solution)/shard_map/reduce-window
  22.6 4.3 %scatter_custom_fusion = s32[1536]{0:T(1024)S(1)} fusion(s32[1024]{0:T(1024)S(1)} %bitcast.150, s32[1024]{0:T(1024)S(1)} %add_select_fusion, s32[]{:T(128)} %constant.30.clone.1), kind=kCustom, calls=%fused_computation.89 | custom fusion | bytes 6148 | tf_op jit(solution)/shard_map/scatter | solution.py:160
  26.9 7.6 %scatter_custom_fusion.1 = bf16[1536]{0:T(1024)(128)(2,1)S(1)} fusion(s32[1024]{0:T(1024)S(1)} %bitcast.151, bf16[1024]{0:T(1024)(128)(2,1)S(1)} %broadcast.163, bf16[]{:T(256)} %constant.82.clone.1), kind=kCustom, calls=%fused_computation.93 | custom fusion | bytes 3074 | tf_op jit(solution)/shard_map/scatter | solution.py:161
  36.5 3.2 gather_fusion
  40.0 14.7 %all_to_all.10 = bf16[16,2,48,128]{3,2,1,0:T(8,128)(2,1)S(1)} all-to-all(bf16[16,2,48,128]{3,2,1,0:T(8,128)(2,1)S(1)} %broadcast_multiply_fusion), channel_id=1, replica_groups=mesh['ep'=16,'tp'=16] {'ep'}, dimensions={0} | all-to-all | bytes 786432 | tf_op jit(solution)/shard_map/all_to_all | solution.py:167
  57.8 1.9 pad_maximum_fusion
  62.5 51.3 %all-gather.5.cloned.1.call-done = bf16[16,2,48,2048]{3,2,0,1:T(8,128)(2,1)} async-done(((bf16[16,2,48,128]{3,2,0,1:T(8,128)(2,1)}), bf16[16,2,48,2048]{3,2,0,1:T(8,128)(2,1)}) %all-gather.5.cloned.1.call-update) | async-done | bytes 6291472 | tf_op jit(solution)/shard_map/all_gather | solution.py:168
  113.8 6.3 %fusion.23 = f32[2,16,48,256]{3,2,1,0:T(8,128)} fusion(bf16[16,2,48,2048]{3,2,0,1:T(8,128)(2,1)} %all-gather.5.cloned.1.call-done, bf16[2,2048,256]{2,1,0:T(8,128)(2,1)} %param.33), kind=kOutput, calls=%fused_computation.40 | convolution fusion | flops 1610612736 | bytes 9961472 | tf_op jit(solution)/shard_map/secd,edf->secf/dot_general | solution.py:169
  120.1 10.0 %convert_bitcast_fusion = bf16[16,2,48,2048]{3,2,0,1:T(8,128)(2,1)} fusion(bf16[2,256,2048]{2,1,0:T(8,128)(2,1)S(1)} %copy-done, f32[2,16,48,256]{3,2,1,0:T(8,128)} %fusion.23, bf16[16,2,48,2048]{3,2,0,1:T(8,128)(2,1)} %all-gather.5.cloned.1.call-done, bf16[2,2048,256]{2,1,0:T(8,128)(2,1)} %param.34), kind=kOutput, calls=%fused_computation.29 | convolution fusion | flops 3226730496 | bytes 18350080 | tf_op jit(solution)/shard_map/secf,efd->secd/dot_general | solution.py:174
  130.1 23.1 %copy.56 = bf16[16,2,48,2048]{2,0,1,3:T(8,128)(2,1)} copy(bf16[16,2,48,2048]{3,2,0,1:T(8,128)(2,1)} %convert_bitcast_fusion) | data formatting | bytes 12582912
  153.2 29.8 %reshape.224 = bf16[2048,1536]{1,0:T(8,128)(2,1)} reshape(bf16[2048,2,16,48]{3,2,1,0:T(8,128)(2,1)} %bitcast.135) | data formatting | bytes 12582912
  183.3 17.5 %all-gather.3.cloned.1.call-done = bf16[8192,544]{1,0:T(8,128)(2,1)} async-done(((bf16[512,544]{1,0:T(8,128)(2,1)}), bf16[8192,544]{1,0:T(8,128)(2,1)}) %all-gather.3.cloned.1.call-update) | async-done | bytes 8912912 | tf_op jit(solution)/shard_map/all_gather | solution.py:14
  200.8 1.6 slice-done
  203.2 7.2 %slice.38 = bf16[8192,512]{1,0:T(8,128)(2,1)} slice(bf16[8192,544]{1,0:T(8,128)(2,1)} %all-gather.3.cloned.1.call-done), slice={[0:8192], [0:512]} | slice | bytes 16777216 | tf_op jit(solution)/shard_map/slice | solution.py:16
  210.4 73.0 %while.15 = (s32[]{:T(128)}, f32[512,2]{0,1:T(2,128)S(1)}, f32[512,2]{0,1:T(2,128)S(1)}, f32[512,2,64]{0,2,1:T(8,128)S(1)}, bf16[16,512,512]{2,1,0:T(8,128)(2,1)...) while((s32[]{:T(128)}, f32[512,2]{0,1:T(2,128)S(1)}, ...), condition=%wide.region_5.6_spmd.clone, body=%wide.region_2.5_spmd.clone.sunk | while | flops 305992704 | bytes 13141125 | solution.py:122
  283.5 3.1 convolution_convert_fusion.2
  286.7 2.1 reshape.225
  288.8 1.8 copy.48
  290.6 5.7 %all-to-all-start.1 = ((bf16[16,2,48,128]{3,2,1,0:T(8,128)(2,1)}), bf16[16,2,48,128]{3,2,1,0:T(8,128)(2,1)S(1)}, u32[]{:S(2)}, u32[]{:S(2)}) async-start(bf16[16,2,48,128]{3,2,1,0:T(8,128)(2,1)} %copy.48), calls=%async_computation.2 | async-start | bytes 786432 | tf_op jit(solution)/shard_map/all_to_all | solution.py:180
  296.5 7.1 %all-to-all-done.1 = bf16[16,2,48,128]{3,2,1,0:T(8,128)(2,1)S(1)} async-done(((bf16[16,2,48,128]{3,2,1,0:T(8,128)(2,1)}), bf16[16,2,48,128]{3,2,1,0:T(8,128)(2,1)S(1)}, u32[]{:S(2)}, u32[]{:S(2)}) %all-to-all-start.1) | async-done | bytes 393248 | tf_op jit(solution)/shard_map/all_to_all | solution.py:180
  303.6 3.2 gather_fusion.1
  306.8 3.5 fusion.37
  310.3 36.6 %reduce-scatter.5.cloned.1.call-done = bf16[32,2048]{1,0:T(8,128)(2,1)} async-done(((bf16[512,2048]{1,0:T(8,128)(2,1)}), bf16[32,2048]{1,0:T(8,128)(2,1)}) %reduce-scatter.5.cloned.1.call-update) | async-done | bytes 131088 | tf_op jit(solution)/shard_map/reduce_scatter | solution.py:136
  (234 shorter events, 83.0 us)
Async XLA Ops:
  7.2 113.0 %copy-start = (bf16[2,256,2048]{2,1,0:T(8,128)(2,1)S(1)}, bf16[2,256,2048]{2,1,0:T(8,128)(2,1)}, u32[]{:S(2)}) copy-start(bf16[2,256,2048]{2,1,0:T(8,128)(2,1)} %param.35) | copy-start | bytes 6291460
  7.2 106.6 %all-gather.5.cloned.1.call-start = ((), (), s32[]{:S(2)}) async-start(), calls=%async_computation.6 | async-start | bytes 6684672 | tf_op jit(solution)/shard_map/all_gather | solution.py:168
  7.2 4.2 %copy-start.2 = (bf16[512,2048]{1,0:T(8,128)(2,1)S(1)}, bf16[512,2048]{1,0:T(8,128)(2,1)}, u32[]{:S(2)}) copy-start(bf16[512,2048]{1,0:T(8,128)(2,1)} %param.29) | copy-start | bytes 6291460
  11.4 0.7 copy-start.11
  39.7 15.9 %copy-start.10 = (bf16[512,32]{0,1:T(8,128)(2,1)S(1)}, bf16[512,32]{0,1:T(8,128)(2,1)}, u32[]{:S(2)}) copy-start(bf16[512,32]{0,1:T(8,128)(2,1)} %param.21) | copy-start | bytes 98308
  39.7 17.7 %copy-start.5 = (bf16[512,512]{1,0:T(8,128)(2,1)S(1)}, bf16[512,512]{1,0:T(8,128)(2,1)}, u32[]{:S(2)}) copy-start(bf16[512,512]{1,0:T(8,128)(2,1)} %param.20) | copy-start | bytes 1572868
  39.7 17.9 %copy-start.13 = (f32[512]{0:T(512)S(1)}, f32[512]{0:T(512)}, u32[]{:S(2)}) copy-start(f32[512]{0:T(512)} %param.23) | copy-start | bytes 6148
  55.5 145.3 %all-gather.3.cloned.1.call-start = ((), (), s32[]{:S(2)}) async-start(), calls=%async_computation.4 | async-start | bytes 11141120 | tf_op jit(solution)/shard_map/all_gather | solution.py:14
  57.6 2.8 copy-start.15
  57.8 2.3 copy-start.6
  59.7 2.1 copy-start.8
  59.7 2.1 copy-start.9
  59.8 226.9 %reduce-scatter.7.cloned.1.call-start = ((), (), s32[]{:S(2)}) async-start(), calls=%async_computation.7 | async-start | bytes 6684672
  60.0 1.9 copy-start.7
  60.0 1.9 copy-start.14
  183.0 163.8 %reduce-scatter.5.cloned.1.call-start = ((), (), s32[]{:S(2)}) async-start(), calls=%async_computation.5 | async-start | bytes 2228224 | tf_op jit(solution)/shard_map/reduce_scatter | solution.py:136
  200.8 1.6 slice-start
  203.2 7.2 %copy-start.3 = (bf16[512,128]{1,0:T(8,128)(2,1)S(1)}, bf16[512,128]{1,0:T(8,128)(2,1)}, u32[]{:S(2)}) copy-start(bf16[512,128]{1,0:T(8,128)(2,1)} %param.26) | copy-start | bytes 393220
  203.2 7.2 %copy-start.4 = (bf16[512,128]{1,0:T(8,128)(2,1)S(1)}, bf16[512,128]{1,0:T(8,128)(2,1)}, u32[]{:S(2)}) copy-start(bf16[512,128]{1,0:T(8,128)(2,1)} %param.27) | copy-start | bytes 393220
  286.6 9.6 %copy-start.12 = (f32[512,2]{0,1:T(2,128)S(1)}, f32[512,2]{0,1:T(2,128)}, u32[]{:S(2)}) copy-start(f32[512,2]{0,1:T(2,128)} %param.32) | copy-start | bytes 12292
  288.8 58.1 %copy-start.1 = (bf16[2,256,2048]{2,1,0:T(8,128)(2,1)S(1)}, bf16[2,256,2048]{2,1,0:T(8,128)(2,1)}, u32[]{:S(2)}) copy-start(bf16[2,256,2048]{2,1,0:T(8,128)(2,1)} %param.35) | copy-start | bytes 6291460
  290.6 13.0 %all-to-all-start.1 = ((bf16[16,2,48,128]{3,2,1,0:T(8,128)(2,1)}), bf16[16,2,48,128]{3,2,1,0:T(8,128)(2,1)S(1)}, u32[]{:S(2)}, u32[]{:S(2)}) async-start(bf16[16,2,48,128]{3,2,1,0:T(8,128)(2,1)} %copy.48), calls=%async_computation.2 | async-start | bytes 786432 | tf_op jit(solution)/shard_map/all_to_all | solution.py:180
Sparse Core Ops, SparseCore 0:
  55.7 58.0 all-gather.4
  116.2 84.5 all-gather.2
  203.4 66.9 reduce-scatter.6
  286.8 60.0 reduce-scatter.4
where the time goes:
time: 356 us; the launch traced here: 353 us
  waiting for transfers between devices  113 us (32%)
  local copies, waits for them, and re-layouts  88.8 us (25%)
  matrix products  88.1 us (25%)
  other arithmetic  27.5 us (8%)
  blocking collectives  14.7 us (4%)
  between operations  14.3 us (4%)
  starting transfers between devices  6.26 us (2%)
    unnamed x38, local copies, waits for them, and re-layouts  56.3 us
    all_gather x1, waiting for transfers between devices, experts(): piece = lax.all_gather(arrived, 'tp', axis=3, tiled=True)  51.3 us
    reduce_scatter x1, waiting for transfers between devices, token_mixer(): lax.psum_scatter(jnp.dot(attended, output_weight, preferred_element_type=...  36.6 us
    dot_general x16, matrix products, scan_step(): jnp.dot(latent_block, value_weight, preferred_element_type=jnp.float32)  21.8 us
    dot_general x16, matrix products, scan_step(): jnp.dot(latent_block, key_weight, preferred_element_type=jnp.float32)  21.7 us
    all_gather x1, waiting for transfers between devices, sent_together(): out, at, outs = (lax.all_gather(both, axis, axis=dim, tiled=True), 0, [])  17.5 us
    all_to_all x1, blocking collectives, experts(): lax.all_to_all(outgoing, 'ep', split_axis=0, concat_axis=0, tiled=True)  14.7 us
    dot_general x1, matrix products, experts(): jnp.einsum('secf,efd->secd', hidden, down_weight, preferred_element_type=...  10 us
  transfers between devices with their start and end apart: 5, of which 4 were waited for; matrix products, arithmetic and copies ran while one was open for 48% of the time, Pallas kernels for 0%

commit v1 on v0

--- a/solution.py
+++ b/solution.py
@@ -165,7 +165,9 @@
         group_count, local_count, capacity, part_width
     )
     arrived = lax.all_to_all(outgoing, "ep", split_axis=0, concat_axis=0, tiled=True)
-    piece = lax.all_gather(arrived, "tp", axis=3, tiled=True)
+    piece = jnp.concatenate(
+        lax.all_to_all(jnp.stack([arrived] * lax.axis_size("tp")), "tp", 0, 0), axis=3
+    )
     gate_running = jnp.einsum(
         "secd,edf->secf", piece, gate_weight, preferred_element_type=jnp.float32
     )

time: 356 us -> 441 us (1.24)
  waiting for transfers between devices: 113 us -> 177 us
  starting transfers between devices: 6.26 us -> 17.6 us
    all_to_all x0 -> x1, waiting for transfers between devices: none -> 137 us  [experts(): lax.all_to_all(jnp.stack([arrived] * lax.axis_size('tp')), 'tp', 0, 0)]
    all_gather x1 -> x0, waiting for transfers between devices: 51.3 us -> none  [experts(): piece = lax.all_gather(arrived, 'tp', axis=3, tiled=True)]
    all_gather x1, waiting for transfers between devices: 17.5 us -> 0.02 us  [sent_together(): out, at, outs = (lax.all_gather(both, axis, axis=dim, tiled=True), 0, [])]
    all_to_all x0 -> x1, starting transfers between devices: none -> 9.72 us  [experts(): lax.all_to_all(jnp.stack([arrived] * lax.axis_size('tp')), 'tp', 0, 0)]
    unnamed x38 -> x26, local copies, waits for them, and re-layouts: 56.3 us -> 56 us
  transfers between devices with their start and end apart: 5 -> 5, of which waited for: 4 -> 3; matrix products, arithmetic and copies ran while one was open for 48% -> 46% of each run, Pallas kernels for 0% -> 0%
where the time goes in v1:
time: 441 us; the launch traced here: 438 us
  waiting for transfers between devices  177 us (40%)
  local copies, waits for them, and re-layouts  91.1 us (21%)
  matrix products  88 us (20%)
  other arithmetic  30.3 us (7%)
  starting transfers between devices  17.6 us (4%)
  blocking collectives  17.4 us (4%)
  between operations  15.9 us (4%)
    all_to_all x1, waiting for transfers between devices, experts(): lax.all_to_all(jnp.stack([arrived] * lax.axis_size('tp')), 'tp', 0, 0)  137 us
    unnamed x26, local copies, waits for them, and re-layouts  56 us
    reduce_scatter x1, waiting for transfers between devices, token_mixer(): lax.psum_scatter(jnp.dot(attended, output_weight, preferred_element_type=...  33.1 us
    dot_general x16, matrix products, scan_step(): jnp.dot(latent_block, value_weight, preferred_element_type=jnp.float32)  21.7 us
    dot_general x16, matrix products, scan_step(): jnp.dot(latent_block, key_weight, preferred_element_type=jnp.float32)  21.7 us
    all_to_all x1, blocking collectives, experts(): lax.all_to_all(outgoing, 'ep', split_axis=0, concat_axis=0, tiled=True)  17.4 us
    dot_general x1, matrix products, experts(): jnp.einsum('secf,efd->secd', hidden, down_weight, preferred_element_type=...  9.94 us
    all_to_all x1, starting transfers between devices, experts(): lax.all_to_all(jnp.stack([arrived] * lax.axis_size('tp')), 'tp', 0, 0)  9.72 us
  transfers between devices with their start and end apart: 5, of which 3 were waited for; matrix products, arithmetic and copies ran while one was open for 46% of the time, Pallas kernels for 0%

profile of v1, /device:TPU:6, one launch (start us, length us, event | category | flops | bytes accessed | tf_op | source)
XLA Modules:
  0.0 438.4 jit_solution(12087460164382789880)
XLA Ops:
  13.4 4.0 convert_element_type.83
  17.5 9.0 %reduce-window.6 = s32[32,8,128]{2,1,0:T(8,128)S(1)} reduce-window(s32[32,8,128]{2,1,0:T(8,128)S(1)} %fusion.54, s32[]{:T(128)} %constant.30.clone.1), window={size=1x1x128 pad=0_0x0_0x127_0}, to_apply=%region_8.9 | reduce-window | flops 4161536 | bytes 262148 | tf_op jit(solution)/shard_map/reduce-window
  27.4 4.3 scatter_custom_fusion
  31.7 7.6 %scatter_custom_fusion.1 = bf16[1536]{0:T(1024)(128)(2,1)S(1)} fusion(s32[1024]{0:T(1024)S(1)} %bitcast.167, bf16[1024]{0:T(1024)(128)(2,1)S(1)} %broadcast.165, bf16[]{:T(256)} %constant.82.clone.1), kind=kCustom, calls=%fused_computation.97 | custom fusion | bytes 3074 | tf_op jit(solution)/shard_map/scatter | solution.py:161
  40.2 2.1 multiply_reduce_fusion
  43.4 3.2 gather_fusion
  46.9 17.4 %all_to_all.15 = bf16[16,2,48,128]{3,2,1,0:T(8,128)(2,1)S(1)} all-to-all(bf16[16,2,48,128]{3,2,1,0:T(8,128)(2,1)S(1)} %broadcast_multiply_fusion), channel_id=1, replica_groups=mesh['ep'=16,'tp'=16] {'ep'}, dimensions={0} | all-to-all | bytes 786432 | tf_op jit(solution)/shard_map/all_to_all | solution.py:167
  64.3 4.1 stack.2
  68.4 9.7 %all-to-all-start.1 = ((bf16[16,16,2,48,128]{4,3,1,2,0:T(8,128)(2,1)}), bf16[16,16,2,48,128]{4,3,1,2,0:T(8,128)(2,1)}, u32[]{:S(2)}, u32[]{:S(2)}) async-start(bf16[16,16,2,48,128]{4,3,1,2,0:T(8,128)(2,1)} %stack.2), calls=%async_computation.2 | async-start | bytes 12582912 | tf_op jit(solution)/shard_map/all_to_all | solution.py:169
  80.8 136.6 %all-to-all-done.1 = bf16[16,16,2,48,128]{4,3,1,2,0:T(8,128)(2,1)} async-done(((bf16[16,16,2,48,128]{4,3,1,2,0:T(8,128)(2,1)}), bf16[16,16,2,48,128]{4,3,1,2,0:T(8,128)(2,1)}, u32[]{:S(2)}, u32[]{:S(2)}) %all-to-all-start.1) | async-done | bytes 6291488 | tf_op jit(solution)/shard_map/all_to_all | solution.py:169
  217.4 6.3 %fusion.19 = f32[2,16,48,256]{3,2,1,0:T(8,128)} fusion(bf16[2,2048,256]{2,1,0:T(8,128)(2,1)} %param.33, bf16[16,16,2,48,128]{4,3,1,2,0:T(8,128)(2,1)} %all-to-all-done.1), kind=kOutput, calls=%fused_computation.31 | convolution fusion | flops 1610612736 | bytes 9961472 | tf_op jit(solution)/shard_map/secd,edf->secf/dot_general | solution.py:171
  223.7 9.9 %convert_bitcast_fusion = bf16[16,2,48,2048]{3,2,0,1:T(8,128)(2,1)} fusion(bf16[2,256,2048]{2,1,0:T(8,128)(2,1)S(1)} %copy-done, f32[2,16,48,256]{3,2,1,0:T(8,128)} %fusion.19, bf16[2,2048,256]{2,1,0:T(8,128)(2,1)} %param.34, bf16[16,16,2,48,128]{4,3,1,2,0:T(8,128)(2,1)} %all-to-all-done.1), kind=kOutput, calls=%fused_computation.33 | convolution fusion | flops 3226730496 | bytes 18350080 | tf_op jit(solution)/shard_map/secf,efd->secd/dot_general | solution.py:176
  233.7 23.1 %copy.57 = bf16[16,2,48,2048]{2,0,1,3:T(8,128)(2,1)} copy(bf16[16,2,48,2048]{3,2,0,1:T(8,128)(2,1)} %convert_bitcast_fusion) | data formatting | bytes 12582912
  256.7 29.7 %reshape.234 = bf16[2048,1536]{1,0:T(8,128)(2,1)} reshape(bf16[2048,2,16,48]{3,2,1,0:T(8,128)(2,1)} %bitcast.151) | data formatting | bytes 12582912
  289.1 7.2 %slice.38 = bf16[8192,512]{1,0:T(8,128)(2,1)} slice(bf16[8192,544]{1,0:T(8,128)(2,1)} %all-gather.2.cloned.1.call-done), slice={[0:8192], [0:512]} | slice | bytes 16777216 | tf_op jit(solution)/shard_map/slice | solution.py:16
  296.3 73.0 %while.15 = (s32[]{:T(128)}, f32[512,2]{0,1:T(2,128)S(1)}, f32[512,2]{0,1:T(2,128)S(1)}, f32[512,2,64]{0,2,1:T(8,128)S(1)}, bf16[16,512,512]{2,1,0:T(8,128)(2,1)...) while((s32[]{:T(128)}, f32[512,2]{0,1:T(2,128)S(1)}, ...), condition=%wide.region_5.6_spmd.clone, body=%wide.region_2.5_spmd.clone.sunk | while | flops 305992704 | bytes 13141125 | solution.py:122
  369.3 3.1 convolution_convert_fusion.2
  372.5 2.1 reshape.235
  374.7 1.8 copy.49
  376.5 7.3 %all-to-all-start.2 = ((bf16[16,2,48,128]{3,2,1,0:T(8,128)(2,1)}), bf16[16,2,48,128]{3,2,1,0:T(8,128)(2,1)S(1)}, u32[]{:S(2)}, u32[]{:S(2)}) async-start(bf16[16,2,48,128]{3,2,1,0:T(8,128)(2,1)} %copy.49), calls=%async_computation.3 | async-start | bytes 786432 | tf_op jit(solution)/shard_map/all_to_all | solution.py:182
  383.9 7.3 %all-to-all-done.2 = bf16[16,2,48,128]{3,2,1,0:T(8,128)(2,1)S(1)} async-done(((bf16[16,2,48,128]{3,2,1,0:T(8,128)(2,1)}), bf16[16,2,48,128]{3,2,1,0:T(8,128)(2,1)S(1)}, u32[]{:S(2)}, u32[]{:S(2)}) %all-to-all-start.2) | async-done | bytes 393248 | tf_op jit(solution)/shard_map/all_to_all | solution.py:182
  391.3 3.2 gather_fusion.1
  394.5 3.5 fusion.45
  397.9 33.1 %reduce-scatter.5.cloned.1.call-done = bf16[32,2048]{1,0:T(8,128)(2,1)} async-done(((bf16[512,2048]{1,0:T(8,128)(2,1)}), bf16[32,2048]{1,0:T(8,128)(2,1)}) %reduce-scatter.5.cloned.1.call-update) | async-done | bytes 131088 | tf_op jit(solution)/shard_map/reduce_scatter | solution.py:136
  (222 shorter events, 85.8 us)
Async XLA Ops:
  8.0 215.7 %copy-start = (bf16[2,256,2048]{2,1,0:T(8,128)(2,1)S(1)}, bf16[2,256,2048]{2,1,0:T(8,128)(2,1)}, u32[]{:S(2)}) copy-start(bf16[2,256,2048]{2,1,0:T(8,128)(2,1)} %param.35) | copy-start | bytes 6291460
  8.0 278.7 %all-gather.2.cloned.1.call-start = ((), (), s32[]{:S(2)}) async-start(), calls=%async_computation.5 | async-start | bytes 11141120 | tf_op jit(solution)/shard_map/all_gather | solution.py:14
  9.0 3.9 copy-start.6
  68.3 10.0 %copy-start.4 = (bf16[512,1024]{1,0:T(8,128)(2,1)S(1)}, bf16[512,1024]{1,0:T(8,128)(2,1)}, u32[]{:S(2)}) copy-start(bf16[512,1024]{1,0:T(8,128)(2,1)} %param.19) | copy-start | bytes 3145732
  68.4 10.3 %copy-start.9 = (f32[1024]{0:T(1024)S(1)}, f32[1024]{0:T(1024)}, u32[]{:S(2)}) copy-start(f32[1024]{0:T(1024)} %param.22) | copy-start | bytes 12292
  68.4 149.0 %all-to-all-start.1 = ((bf16[16,16,2,48,128]{4,3,1,2,0:T(8,128)(2,1)}), bf16[16,16,2,48,128]{4,3,1,2,0:T(8,128)(2,1)}, u32[]{:S(2)}, u32[]{:S(2)}) async-start(bf16[16,16,2,48,128]{4,3,1,2,0:T(8,128)(2,1)} %stack.2), calls=%async_computation.2 | async-start | bytes 12582912 | tf_op jit(solution)/shard_map/all_to_all | solution.py:169
  78.1 294.4 %reduce-scatter.7.cloned.1.call-start = ((), (), s32[]{:S(2)}) async-start(), calls=%async_computation.7 | async-start | bytes 6684672
  78.4 1.9 copy-start.5
  78.4 1.8 copy-start.8
  286.4 144.6 %reduce-scatter.5.cloned.1.call-start = ((), (), s32[]{:S(2)}) async-start(), calls=%async_computation.6 | async-start | bytes 2228224 | tf_op jit(solution)/shard_map/reduce_scatter | solution.py:136
  286.7 1.6 slice-start
  289.1 7.2 %copy-start.2 = (bf16[512,128]{1,0:T(8,128)(2,1)S(1)}, bf16[512,128]{1,0:T(8,128)(2,1)}, u32[]{:S(2)}) copy-start(bf16[512,128]{1,0:T(8,128)(2,1)} %param.26) | copy-start | bytes 393220
  289.1 7.2 %copy-start.3 = (bf16[512,128]{1,0:T(8,128)(2,1)S(1)}, bf16[512,128]{1,0:T(8,128)(2,1)}, u32[]{:S(2)}) copy-start(bf16[512,128]{1,0:T(8,128)(2,1)} %param.27) | copy-start | bytes 393220
  372.5 11.3 %copy-start.7 = (f32[512,2]{0,1:T(2,128)S(1)}, f32[512,2]{0,1:T(2,128)}, u32[]{:S(2)}) copy-start(f32[512,2]{0,1:T(2,128)} %param.32) | copy-start | bytes 12292
  374.6 56.3 %copy-start.1 = (bf16[2,256,2048]{2,1,0:T(8,128)(2,1)S(1)}, bf16[2,256,2048]{2,1,0:T(8,128)(2,1)}, u32[]{:S(2)}) copy-start(bf16[2,256,2048]{2,1,0:T(8,128)(2,1)} %param.35) | copy-start | bytes 6291460
  376.5 14.8 %all-to-all-start.2 = ((bf16[16,2,48,128]{3,2,1,0:T(8,128)(2,1)}), bf16[16,2,48,128]{3,2,1,0:T(8,128)(2,1)S(1)}, u32[]{:S(2)}, u32[]{:S(2)}) async-start(bf16[16,2,48,128]{3,2,1,0:T(8,128)(2,1)} %copy.49), calls=%async_computation.3 | async-start | bytes 786432 | tf_op jit(solution)/shard_map/all_to_all | solution.py:182
Sparse Core Ops, SparseCore 0:
  13.0 91.0 all-gather.1
Sparse Core Ops, SparseCore 1:
  286.5 65.5 reduce-scatter.6
  372.6 58.3 reduce-scatter.4
